TPU v7x, 32 devices: a whole 2x2x4 slice. The times are simulated.
32 devices in a mesh: sp: 16 (over z, y, x), tp: 2 (over core).
Axes of the slice: x: 2, y: 2, z: 4, core: 2. Of those that a mesh axis runs over, the one named last changes fastest.
Arguments:
- queries: bfloat16 [4096, 8, 128], P('sp', 'tp'), may hold values from -6 to 6
- keys: bfloat16 [4096, 2, 128], P('sp'), may hold values from -6 to 6
- values: bfloat16 [4096, 2, 128], P('sp'), may hold values from -6 to 6
- documents: int32 [4096], P('sp'), may hold values from 0 to 3, never falling along the last dimension, each value on 1 to 2304 neighbouring positions
- query_gain: float32 [128], replicated, may hold values from 0.25 to 4
- key_gain: float32 [128], replicated, may hold values from 0.25 to 4
- out_weight: bfloat16 [1024, 2048], P('tp'), may hold values from -0.1875 to 0.1875
- residual: bfloat16 [4096, 2048], P('sp'), may hold values from -6 to 6
- norm_gain: float32 [2048], replicated, may hold values from 0.1 to 1.9
- up_weight: bfloat16 [2048, 6144], P('sp', 'tp'), may hold values from -0.125 to 0.125
- down_weight: bfloat16 [2048, 6144], P('sp', 'tp'), may hold values from -0.078125 to 0.078125
Outputs:
- layer_out: bfloat16 [4096, 2048], P(('sp', 'tp'))
Inputs may be any that keep to these rules, and one draw needn't show every extreme that they name: `documents`: document numbers never fall along the sequence; one document covers exactly (9) * 256 positions.
All inputs are finite; a program needn't handle non-finite values.
Results may differ from a plain program's by a relative error of at most 0.017.
Values may be sent and summed in bfloat16 or wider, within the bound.
No kernel may reach another device: no remote copies, remote signals or barrier semaphores. Data moves between devices by JAX's collectives and lax.ppermute only.
A program may use at most 128 MiB of HBM per device.

v0:
```python
import jax
import jax.numpy as jnp
from jax import lax
from jax.sharding import PartitionSpec as P

QUERY_HEADS = 8
GRID = 64
EPS = 1e-06
THETA = 10000.0


def head_norm(block, gain):
    return block * lax.rsqrt(jnp.mean(block * block, axis=-1, keepdims=True) + EPS) * gain


def rotate(block, positions):
    head_width = block.shape[-1]
    pair_count = head_width // 4
    inverse = THETA ** (-jnp.arange(pair_count, dtype=jnp.float32) / pair_count)
    grid_row = (positions // GRID).astype(jnp.float32)[:, None] * inverse
    grid_col = (positions % GRID).astype(jnp.float32)[:, None] * inverse
    angles = jnp.concatenate([grid_row, grid_row, grid_col, grid_col], axis=-1)
    cosine = jnp.cos(angles)[:, None, :]
    sine_table = jnp.sin(angles)[:, None, :]
    turned = jnp.concatenate(
        [
            -block[..., pair_count : 2 * pair_count],
            block[..., 0:pair_count],
            -block[..., 3 * pair_count :],
            block[..., 2 * pair_count : 3 * pair_count],
        ],
        axis=-1,
    )
    return block * cosine + turned * sine_table


def channel_norm(rows_in, gain):
    widened = rows_in.astype(jnp.float32)
    return (
        widened * lax.rsqrt(jnp.mean(widened * widened, axis=-1, keepdims=True) + EPS) * gain
    ).astype(jnp.bfloat16)


def body(
    queries,
    keys,
    values,
    documents,
    query_gain,
    key_gain,
    out_weight,
    residual,
    norm_gain,
    up_weight,
    down_weight,
):
    tok_dev = queries.shape[0]
    heads_here = queries.shape[1]
    head_width = queries.shape[2]
    query_group_count = QUERY_HEADS // keys.shape[1]
    kv_index = lax.axis_index("tp") * heads_here // query_group_count
    positions = lax.axis_index("sp") * tok_dev + jnp.arange(tok_dev, dtype=jnp.int32)
    own_keys = lax.dynamic_index_in_dim(keys, kv_index, 1, keepdims=True)
    own_values = lax.dynamic_index_in_dim(values, kv_index, 1, keepdims=False)
    key_rot = rotate(head_norm(own_keys.astype(jnp.float32), key_gain), positions)[:, 0, :].astype(
        jnp.bfloat16
    )
    rotated_query = rotate(head_norm(queries.astype(jnp.float32), query_gain), positions).astype(
        jnp.bfloat16
    )
    scale = head_width ** (-0.5)
    first_doc = documents[0]
    last_doc = documents[tok_dev - 1]
    start_state = (
        jnp.full((tok_dev, heads_here), -1e30, jnp.float32),
        jnp.zeros((tok_dev, heads_here), jnp.float32),
        jnp.zeros((tok_dev, heads_here, head_width), jnp.float32),
    )
    piece_keys = lax.all_gather(key_rot, "sp", axis=0, tiled=True)
    piece_values = lax.all_gather(own_values, "sp", axis=0, tiled=True)
    piece_docs = lax.all_gather(documents, "sp", axis=0, tiled=True)

    def update(state):
        peak, denom, summed = state
        scores = (
            jnp.einsum("qhd,kd->qhk", rotated_query, piece_keys, preferred_element_type=jnp.float32)
            * scale
        )
        allowed = (documents[:, None] == piece_docs[None, :])[:, None, :]
        scores = jnp.where(allowed, scores, -1e30)
        new_peak = jnp.maximum(peak, jnp.max(scores, axis=-1))
        probs = jnp.where(allowed, jnp.exp(scores - new_peak[..., None]), 0.0)
        denom = jnp.sum(probs, axis=-1)
        summed = jnp.einsum(
            "qhk,kd->qhd",
            probs.astype(jnp.bfloat16),
            piece_values,
            preferred_element_type=jnp.float32,
        )
        return (new_peak, denom, summed)

    touches = jnp.logical_and(
        piece_docs[0] <= last_doc, piece_docs[piece_docs.shape[0] - 1] >= first_doc
    )
    peak, denom, summed = lax.cond(touches, update, lambda state: state, start_state)
    attn = (
        (summed / denom[..., None]).reshape(tok_dev, heads_here * head_width).astype(jnp.bfloat16)
    )
    share = tok_dev // lax.axis_size("tp")
    branch = lax.psum(
        jnp.dot(attn, out_weight, preferred_element_type=jnp.float32).astype(jnp.bfloat16), "tp"
    ).astype(jnp.float32)
    whole_rows = (residual.astype(jnp.float32) + branch).astype(jnp.bfloat16)
    normed = channel_norm(whole_rows, norm_gain)
    mid = lax.dynamic_slice_in_dim(whole_rows, lax.axis_index("tp") * share, share, 0)
    raised = jnp.dot(
        normed,
        lax.all_gather(up_weight, "sp", axis=0, tiled=True),
        preferred_element_type=jnp.float32,
    )
    hidden = jnp.square(jax.nn.relu(raised)).astype(jnp.bfloat16)
    terms = lax.dot_general(
        hidden,
        lax.all_gather(down_weight, "sp", axis=0, tiled=True),
        (((1,), (1,)), ((), ())),
        preferred_element_type=jnp.float32,
    )
    mixer = lax.psum_scatter(
        terms.astype(jnp.bfloat16), "tp", scatter_dimension=0, tiled=True
    ).astype(jnp.float32)
    return (mid.astype(jnp.float32) + mixer).astype(jnp.bfloat16)


def solution(mesh):
    in_specs = (
        P("sp", "tp", None),
        P("sp", None, None),
        P("sp", None, None),
        P("sp"),
        P(),
        P(),
        P("tp", None),
        P("sp", None),
        P(),
        P("sp", "tp"),
        P("sp", "tp"),
    )
    out_specs = P(("sp", "tp"), None)
    return jax.shard_map(body, mesh=mesh, in_specs=in_specs, out_specs=out_specs, check_vma=False)
```

profile of v0, /device:TPU:0, one launch (start us, length us, event | category | flops | bytes accessed | tf_op | source)
XLA Modules:
  0.0 500.5 jit_solution(8802338885907431787)
XLA Ops:
  6.6 1.2 constant_dynamic-slice_fusion.1
  7.9 0.8 fusion.27
  9.0 1.9 fusion.29
  11.0 1.0 constant_dynamic-slice_fusion
  12.7 42.7 %all-gather.2 = s32[16,1,256]{2,1,0:T(1,128)S(1)} all-gather(s32[1,1,256]{2,1,0:T(1,128)} %bitcast.27), channel_id=1, replica_groups=mesh['sp'=16,'tp'=2] {'sp'}, dimensions={0}, use_global_device_ids=true | all-gather | bytes 17408 | tf_op jit(solution)/shard_map/all_gather | solution.py:81
  55.5 1.3 fusion.39
  56.8 0.7 fusion.38
  60.6 1.2 fusion.22
  61.8 1.2 fusion.23
  63.4 1.6 fusion.25
  65.0 3.9 all-gather.12.cloned.1.call-done
  68.9 56.7 %all-gather.14.cloned.1.call-done = bf16[4096,1,128]{2,0,1:T(8,128)(2,1)} async-done(((bf16[256,1,128]{2,0,1:T(8,128)(2,1)}), bf16[4096,1,128]{2,0,1:T(8,128)(2,1)}) %all-gather.14.cloned.1.call-update) | async-done | bytes 1048592 | tf_op jit(solution)/shard_map/all_gather | solution.py:80
  125.6 15.6 %conditional.1 = (f32[256,4]{0,1:T(4,128)S(1)}, f32[256,4,128]{0,2,1:T(8,128)S(1)}) conditional(s32[]{:T(128)} %bitcast.4, () %tuple.13, (s32[256]{0:T(256)S(1)}, s32[4096]{0:T(1024)S(1)}, bf16[256,4,128]{2,0,1:T(8,128)(2,1)S(1)}, bf16[4096,128]{1,0:T(8,128)(2,1)}, bf16[4096,128]{1,0:T(8,128)(2,1)}) %tuple.50), branch_computations={%region_2.3_spmd, %region_3.6_spmd} | conditional | flops 2203057152 | bytes 61645868 | solution.py:105
  126.3 4.8 fusion
  131.1 4.9 fusion.3
  136.0 5.1 %fusion.2 = f32[256,4]{0,1:T(4,128)S(1)} fusion(f32[256,4,4096]{2,0,1:T(8,128)S(1)} %get-tuple-element.28, f32[256,4]{0,1:T(4,128)S(1)} %broadcast_maximum_fusion, pred[256,4096]{1,0:T(8,128)(4,1)S(1)} %broadcast_compare_fusion), kind=kLoop, calls=%fused_computation.4 | loop fusion | flops 20970496 | bytes 17833984 | tf_op jit(solution)/shard_map/cond/branch_1_fun/reduce_sum | solution.py:93
  141.3 1.7 convolution_convert_fusion
  144.2 17.2 %all-reduce.2.cloned.1.call-done = bf16[256,2048]{1,0:T(8,128)(2,1)} async-done(((bf16[256,2048]{1,0:T(8,128)(2,1)}), bf16[256,2048]{1,0:T(8,128)(2,1)}) %all-reduce.2.cloned.1.call-update) | async-done | bytes 1048592 | tf_op jit(solution)/shard_map/psum | solution.py:110
  161.4 2.0 fusion.14
  163.5 153.2 %all-gather.10.cloned.1.call-done = bf16[2048,3072]{1,0:T(8,128)(2,1)} async-done(((bf16[128,3072]{1,0:T(8,128)(2,1)}), bf16[2048,3072]{1,0:T(8,128)(2,1)}) %all-gather.10.cloned.1.call-update) | async-done | bytes 12582928 | tf_op jit(solution)/shard_map/all_gather | solution.py:124
  316.7 152.3 %all-gather.8.cloned.1.call-done = bf16[2048,3072]{1,0:T(8,128)(2,1)} async-done(((bf16[128,3072]{1,0:T(8,128)(2,1)}), bf16[2048,3072]{1,0:T(8,128)(2,1)}) %all-gather.8.cloned.1.call-update) | async-done | bytes 12582928 | tf_op jit(solution)/shard_map/all_gather | solution.py:118
  468.9 16.0 %convolution_convert_fusion.1 = bf16[256,2048]{1,0:T(8,128)(2,1)} fusion(bf16[2048,3072]{1,0:T(8,128)(2,1)} %all-gather.10.cloned.1.call-done, bf16[2048,3072]{1,0:T(8,128)(2,1)} %all-gather.8.cloned.1.call-done, bf16[256,2048]{1,0:T(8,128)(2,1)S(1)} %get-tuple-element.26, f32[2048]{0:T(1024)S(1)} %copy-done.3, f32[256]{0:T(256)S(1)} %add_rsqrt_fusion.1), kind=kOutput, calls=%fused_computation.21 | convolution fusion | flops 6447431680 | bytes 27272192 | tf_op jit(solution)/shard_map/dot_general | solution.py:122
  485.0 6.7 %reduce-scatter.2.cloned.1.call-done = bf16[128,2048]{1,0:T(8,128)(2,1)} async-done(((bf16[256,2048]{1,0:T(8,128)(2,1)}), bf16[128,2048]{1,0:T(8,128)(2,1)}) %reduce-scatter.2.cloned.1.call-update) | async-done | bytes 524304 | tf_op jit(solution)/shard_map/reduce_scatter | solution.py:128
  491.7 2.0 add_convert_fusion.1
  (34 shorter events, 4.2 us)
Async XLA Ops:
  6.5 134.7 %copy-start = (bf16[512,2048]{1,0:T(8,128)(2,1)S(1)}, bf16[512,2048]{1,0:T(8,128)(2,1)}, u32[]{:S(2)}) copy-start(bf16[512,2048]{1,0:T(8,128)(2,1)} %param.19) | copy-start | bytes 6291460
  6.5 119.1 %copy-start.1 = (s32[256]{0:T(256)S(1)}, s32[256]{0:T(256)}, u32[]{:S(2)}) copy-start(s32[256]{0:T(256)} %param.16) | copy-start | bytes 3076
  6.5 62.3 %all-gather.12.cloned.1.call-start = ((), (), s32[]{:S(2)}) async-start(), calls=%async_computation.5 | async-start | bytes 1114112 | tf_op jit(solution)/shard_map/all_gather | solution.py:79
  10.9 114.7 %all-gather.14.cloned.1.call-start = ((), (), s32[]{:S(2)}) async-start(), calls=%async_computation.6 | async-start | bytes 1114112 | tf_op jit(solution)/shard_map/all_gather | solution.py:80
  12.7 148.7 %all-reduce.2.cloned.1.call-start = ((), (), s32[]{:S(2)}) async-start(), calls=%async_computation.1 | async-start | bytes 2097152 | tf_op jit(solution)/shard_map/psum | solution.py:110
  125.6 343.3 %copy-start.3 = (f32[2048]{0:T(1024)S(1)}, f32[2048]{0:T(1024)}, u32[]{:S(2)}) copy-start(f32[2048]{0:T(1024)} %param.21) | copy-start | bytes 24580
  126.3 4.8 copy-start.2
  143.0 173.7 %all-gather.10.cloned.1.call-start = ((), (), s32[]{:S(2)}) async-start(), calls=%async_computation.3 | async-start | bytes 13369344 | tf_op jit(solution)/shard_map/all_gather | solution.py:124
  143.6 325.3 %all-gather.8.cloned.1.call-start = ((), (), s32[]{:S(2)}) async-start(), calls=%async_computation.2 | async-start | bytes 13369344 | tf_op jit(solution)/shard_map/all_gather | solution.py:118
  144.2 347.5 %reduce-scatter.2.cloned.1.call-start = ((), (), s32[]{:S(2)}) async-start(), calls=%async_computation.4 | async-start | bytes 1572864 | tf_op jit(solution)/shard_map/reduce_scatter | solution.py:128
Sparse Core Ops, SparseCore 0:
  11.0 57.7 all-gather.11
  71.6 53.9 all-gather.13
  143.1 18.2 all-reduce.1
  164.0 152.5 all-gather.9
  319.3 149.5 all-gather.7
  485.1 6.5 reduce-scatter.1
where the time goes:
time: 501 us
  waiting for transfers between devices  391 us (78%)
  blocking collectives  42.7 us (9%)
  matrix products  27.4 us (5%)
  other arithmetic  17.9 us (4%)
  between operations  16.1 us (3%)
    all_gather x1, waiting for transfers between devices, body(): lax.all_gather(down_weight, 'sp', axis=0, tiled=True)  153 us
    all_gather x1, waiting for transfers between devices, body(): lax.all_gather(up_weight, 'sp', axis=0, tiled=True)  152 us
    all_gather x1, waiting for transfers between devices, body(): piece_values = lax.all_gather(own_values, 'sp', axis=0, tiled=True)  56.7 us
    all_gather x1, blocking collectives, body(): piece_docs = lax.all_gather(documents, 'sp', axis=0, tiled=True)  42.7 us
    psum x1, waiting for transfers between devices, body(): lax.psum(jnp.dot(attn, out_weight, preferred_element_type=jnp.float32).as...  17.2 us
    dot_general x1, matrix products, body(): lax.dot_general(hidden, lax.all_gather(down_weight, 'sp', axis=0, tiled=T...  16 us
  transfers between devices with their start and end apart: 6, of which 6 were waited for; matrix products, arithmetic and copies ran while one was open for 2% of the time, Pallas kernels for 0%

commit v1 on v0

--- a/solution.py
+++ b/solution.py
@@ -76,8 +76,11 @@
         jnp.zeros((tok_dev, heads_here), jnp.float32),
         jnp.zeros((tok_dev, heads_here, head_width), jnp.float32),
     )
-    piece_keys = lax.all_gather(key_rot, "sp", axis=0, tiled=True)
-    piece_values = lax.all_gather(own_values, "sp", axis=0, tiled=True)
+    piece_keys, piece_values = jnp.split(
+        lax.all_gather(jnp.concatenate([key_rot, own_values], axis=1), "sp", axis=0, tiled=True),
+        [key_rot.shape[1]],
+        axis=1,
+    )
     piece_docs = lax.all_gather(documents, "sp", axis=0, tiled=True)
 
     def update(state):

time: 501 us -> 450 us (0.90)
  waiting for transfers between devices: 391 us -> 342 us
    all_gather x2 -> x1, waiting for transfers between devices: 60.6 us -> 10.9 us  [body(): lax.all_gather(jnp.concatenate([key_rot, own_values], axis=1), 'sp', axis...]
  transfers between devices with their start and end apart: 6 -> 5, of which waited for: 6 -> 5; matrix products, arithmetic and copies ran while one was open for 2% -> 2% of each run, Pallas kernels for 0% -> 0%
where the time goes in v1:
time: 450 us; the launch traced here: 449 us
  waiting for transfers between devices  342 us (76%)
  blocking collectives  42.7 us (9%)
  matrix products  27.5 us (6%)
  other arithmetic  17.9 us (4%)
  between operations  15.8 us (4%)
    all_gather x1, waiting for transfers between devices, body(): lax.all_gather(up_weight, 'sp', axis=0, tiled=True)  153 us
    all_gather x1, waiting for transfers between devices, body(): lax.all_gather(down_weight, 'sp', axis=0, tiled=True)  152 us
    all_gather x1, blocking collectives, body(): piece_docs = lax.all_gather(documents, 'sp', axis=0, tiled=True)  42.7 us
    psum x1, waiting for transfers between devices, body(): lax.psum(jnp.dot(attn, out_weight, preferred_element_type=jnp.float32).as...  17 us
    dot_general x1, matrix products, body(): lax.dot_general(hidden, lax.all_gather(down_weight, 'sp', axis=0, tiled=T...  16 us
    all_gather x1, waiting for transfers between devices, body(): lax.all_gather(jnp.concatenate([key_rot, own_values], axis=1), 'sp', axis...  10.9 us
  transfers between devices with their start and end apart: 5, of which 5 were waited for; matrix products, arithmetic and copies ran while one was open for 2% of the time, Pallas kernels for 0%

profile of v1, /device:TPU:0, one launch (start us, length us, event | category | flops | bytes accessed | tf_op | source)
XLA Modules:
  0.0 449.3 jit_solution(15470265560838712947)
XLA Ops:
  6.6 1.4 constant_dynamic-slice_fusion
  8.1 0.8 fusion.29
  9.2 1.3 fusion.32
  10.5 0.7 pad_maximum_fusion.1
  11.2 42.7 %all-gather = s32[16,1,256]{2,1,0:T(1,128)S(1)} all-gather(s32[1,1,256]{2,1,0:T(1,128)} %bitcast.30), channel_id=1, replica_groups=mesh['sp'=16,'tp'=2] {'sp'}, dimensions={0}, use_global_device_ids=true | all-gather | bytes 17408 | tf_op jit(solution)/shard_map/all_gather | solution.py:84
  54.0 1.4 fusion.42
  59.1 1.2 fusion.24
  60.3 1.2 fusion.25
  61.9 1.6 fusion.27
  63.5 10.9 %all-gather.5.cloned.1.call-done = bf16[4096,256]{1,0:T(8,128)(2,1)} async-done(((bf16[256,256]{1,0:T(8,128)(2,1)}), bf16[4096,256]{1,0:T(8,128)(2,1)}) %all-gather.5.cloned.1.call-update) | async-done | bytes 2097168 | tf_op jit(solution)/shard_map/all_gather | solution.py:80
  74.4 15.7 %conditional.1 = (f32[256,4]{0,1:T(4,128)S(1)}, f32[256,4,128]{0,2,1:T(8,128)S(1)}) conditional(s32[]{:T(128)} %bitcast.4, () %tuple.13, (s32[256]{0:T(256)S(1)}, s32[4096]{0:T(1024)S(1)}, bf16[4096,256]{1,0:T(8,128)(2,1)}, bf16[256,4,128]{2,0,1:T(8,128)(2,1)S(1)}) %tuple.47), branch_computations={%region_2.3_spmd, %region_3.6_spmd} | conditional | flops 2203057152 | bytes 65840172 | solution.py:108
  74.4 0.6 broadcast_compare_fusion
  75.1 4.9 %fusion = (f32[256,4]{0,1:T(4,128)S(1)}, f32[256,4,4096]{2,0,1:T(8,128)S(1)}) fusion(pred[256,4096]{1,0:T(8,128)(4,1)S(1)} %broadcast_compare_fusion, bf16[256,4,128]{2,0,1:T(8,128)(2,1)S(1)} %get-tuple-element.18, bf16[4096,256]{1,0:T(8,128)(2,1)} %get-tuple-element.19), kind=kOutput, calls=%fused_computation.2 | convolution fusion | flops 1086323712 | bytes 19140608 | tf_op jit(solution)/shard_map/cond/branch_1_fun/qhd,kd->qhk/dot_general | solution.py:89
  80.0 4.9 %fusion.3 = f32[256,4,128]{0,2,1:T(8,128)S(1)} fusion(f32[256,4,4096]{2,0,1:T(8,128)S(1)} %get-tuple-element.28, f32[256,4]{0,1:T(4,128)S(1)} %broadcast_maximum_fusion, pred[256,4096]{1,0:T(8,128)(4,1)S(1)} %broadcast_compare_fusion, bf16[4096,256]{1,0:T(8,128)(2,1)S(1)} %copy-done.2), kind=kOutput, calls=%fused_computation.5 | convolution fusion | flops 1094713344 | bytes 19402752 | tf_op jit(solution)/shard_map/cond | solution.py:108
  84.9 5.1 %fusion.2 = f32[256,4]{0,1:T(4,128)S(1)} fusion(f32[256,4,4096]{2,0,1:T(8,128)S(1)} %get-tuple-element.28, f32[256,4]{0,1:T(4,128)S(1)} %broadcast_maximum_fusion, pred[256,4096]{1,0:T(8,128)(4,1)S(1)} %broadcast_compare_fusion), kind=kLoop, calls=%fused_computation.4 | loop fusion | flops 20970496 | bytes 17833984 | tf_op jit(solution)/shard_map/cond/branch_1_fun/reduce_sum | solution.py:96
  90.3 1.7 convolution_convert_fusion
  92.0 0.7 all-gather.7.cloned.1.call-update
  93.3 17.0 %all-reduce.2.cloned.1.call-done = bf16[256,2048]{1,0:T(8,128)(2,1)} async-done(((bf16[256,2048]{1,0:T(8,128)(2,1)}), bf16[256,2048]{1,0:T(8,128)(2,1)}) %all-reduce.2.cloned.1.call-update) | async-done | bytes 1048592 | tf_op jit(solution)/shard_map/psum | solution.py:113
  110.4 2.0 fusion.16
  112.4 153.4 %all-gather.7.cloned.1.call-done = bf16[2048,3072]{1,0:T(8,128)(2,1)} async-done(((bf16[128,3072]{1,0:T(8,128)(2,1)}), bf16[2048,3072]{1,0:T(8,128)(2,1)}) %all-gather.7.cloned.1.call-update) | async-done | bytes 12582928 | tf_op jit(solution)/shard_map/all_gather | solution.py:121
  265.8 152.3 %all-gather.9.cloned.1.call-done = bf16[2048,3072]{1,0:T(8,128)(2,1)} async-done(((bf16[128,3072]{1,0:T(8,128)(2,1)}), bf16[2048,3072]{1,0:T(8,128)(2,1)}) %all-gather.9.cloned.1.call-update) | async-done | bytes 12582928 | tf_op jit(solution)/shard_map/all_gather | solution.py:127
  418.0 16.0 %convolution_convert_fusion.1 = bf16[256,2048]{1,0:T(8,128)(2,1)} fusion(bf16[2048,3072]{1,0:T(8,128)(2,1)} %all-gather.9.cloned.1.call-done, bf16[2048,3072]{1,0:T(8,128)(2,1)} %all-gather.7.cloned.1.call-done, bf16[256,2048]{1,0:T(8,128)(2,1)S(1)} %get-tuple-element.26, f32[2048]{0:T(1024)S(1)} %copy-done.3, f32[256]{0:T(256)S(1)} %add_rsqrt_fusion.1), kind=kOutput, calls=%fused_computation.23 | convolution fusion | flops 6447431680 | bytes 27272192 | tf_op jit(solution)/shard_map/dot_general | solution.py:125
  434.1 6.7 %reduce-scatter.2.cloned.1.call-done = bf16[128,2048]{1,0:T(8,128)(2,1)} async-done(((bf16[256,2048]{1,0:T(8,128)(2,1)}), bf16[128,2048]{1,0:T(8,128)(2,1)}) %reduce-scatter.2.cloned.1.call-update) | async-done | bytes 524304 | tf_op jit(solution)/shard_map/reduce_scatter | solution.py:131
  440.8 2.0 add_convert_fusion.1
  (31 shorter events, 2.9 us)
Async XLA Ops:
  6.5 83.7 %copy-start = (bf16[512,2048]{1,0:T(8,128)(2,1)S(1)}, bf16[512,2048]{1,0:T(8,128)(2,1)}, u32[]{:S(2)}) copy-start(bf16[512,2048]{1,0:T(8,128)(2,1)} %param.19) | copy-start | bytes 6291460
  6.5 67.9 %copy-start.1 = (s32[256]{0:T(256)S(1)}, s32[256]{0:T(256)}, u32[]{:S(2)}) copy-start(s32[256]{0:T(256)} %param.16) | copy-start | bytes 3076
  6.5 67.9 %all-gather.5.cloned.1.call-start = ((), (), s32[]{:S(2)}) async-start(), calls=%async_computation.1 | async-start | bytes 2228224 | tf_op jit(solution)/shard_map/all_gather | solution.py:80
  11.2 99.2 %all-reduce.2.cloned.1.call-start = ((), (), s32[]{:S(2)}) async-start(), calls=%async_computation.2 | async-start | bytes 2097152 | tf_op jit(solution)/shard_map/psum | solution.py:113
  74.4 343.6 %copy-start.3 = (f32[2048]{0:T(1024)S(1)}, f32[2048]{0:T(1024)}, u32[]{:S(2)}) copy-start(f32[2048]{0:T(1024)} %param.21) | copy-start | bytes 24580
  75.1 4.9 %copy-start.2 = (bf16[4096,256]{1,0:T(8,128)(2,1)S(1)}, bf16[4096,256]{1,0:T(8,128)(2,1)}, u32[]{:S(2)}) copy-start(bf16[4096,256]{1,0:T(8,128)(2,1)} %get-tuple-element.19) | copy-start | bytes 6291460 | tf_op jit(solution)/shard_map/cond
  92.0 173.8 %all-gather.7.cloned.1.call-start = ((), (), s32[]{:S(2)}) async-start(), calls=%async_computation.3 | async-start | bytes 13369344 | tf_op jit(solution)/shard_map/all_gather | solution.py:121
  92.7 325.3 %all-gather.9.cloned.1.call-start = ((), (), s32[]{:S(2)}) async-start(), calls=%async_computation.4 | async-start | bytes 13369344 | tf_op jit(solution)/shard_map/all_gather | solution.py:127
  93.3 347.5 %reduce-scatter.2.cloned.1.call-start = ((), (), s32[]{:S(2)}) async-start(), calls=%async_computation.5 | async-start | bytes 1572864 | tf_op jit(solution)/shard_map/reduce_scatter | solution.py:131
Sparse Core Ops, SparseCore 0:
  11.3 63.0 all-gather.4
  92.1 18.2 all-reduce.1
  113.1 152.5 all-gather.6
  268.4 149.5 all-gather.8
  434.2 6.5 reduce-scatter.1
